TPU v7x, 32 devices: a whole 2x2x4 slice. The times are simulated.
32 devices in a mesh: sp: 4 (over y, core), dp: 8 (over z, x).
Axes of the slice: x: 2, y: 2, z: 4, core: 2. Of those that a mesh axis runs over, the one named last changes fastest.
Arguments:
- queries: bfloat16 [8, 704, 2048], P('dp', 'sp'), may hold values from -24 to 24, as said below
- keys: bfloat16 [8, 704, 256], P('dp', 'sp'), may hold values from -24 to 24, as said below
- tokens: bfloat16 [8, 704, 2304], P('dp', 'sp'), may hold values from -18 to 18
- w_value: bfloat16 [2304, 256], P('dp'), may hold values from -0.125 to 0.125
- q_gain: float32 [128], replicated, may hold values from 0.5 to 6, as said below
- k_gain: float32 [128], replicated, may hold values from 0.5 to 6, as said below
Outputs:
- attended: bfloat16 [8, 704, 2048], P('dp', 'sp')
Inputs may be any that keep to these rules, and one draw needn't show every extreme that they name: `queries`: real-valued projected query entries. `keys`: real-valued projected key entries. `q_gain`: positive gains. `k_gain`: positive gains.
All inputs are finite; a program needn't handle non-finite values.
Results may differ from a plain program's by a relative error of at most 0.0022.
The roundings to bfloat16 on the way count: a program that leaves them out, or rounds other values in their place, can miss the bound.
Values may be sent and summed in bfloat16 or wider, within the bound.
A program may use at most 64 MiB of HBM per device.

v0:
```python
import math

import jax
import jax.numpy as jnp
from jax import lax
from jax.sharding import PartitionSpec as P

HD = 128
QH = 16
KVH = 2
GRID_W = 64


epsilon = 1e-06


def unit_rms(vectors, scaling):
    return (
        vectors * lax.rsqrt(jnp.mean(vectors * vectors, axis=-1, keepdims=True) + epsilon) * scaling
    )


def rotary(vectors, row_pos, col_pos):
    head_width = vectors.shape[-1]
    half_width = head_width // 2
    quarter = half_width // 2
    frequency = 10000.0 ** (-jnp.arange(quarter, dtype=jnp.float32) * 2.0 / half_width)

    def rotate_half(section, angle_pos):
        angles = angle_pos[:, None, None] * frequency
        cosine = jnp.cos(angles)
        sine_table = jnp.sin(angles)
        leading = section[..., :quarter]
        second = section[..., quarter:]
        return jnp.concatenate(
            [leading * cosine - second * sine_table, second * cosine + leading * sine_table],
            axis=-1,
        )

    return jnp.concatenate(
        [
            rotate_half(vectors[..., :half_width], row_pos),
            rotate_half(vectors[..., half_width:], col_pos),
        ],
        axis=-1,
    )


def attend(query_heads, key_heads, value_heads):
    length, item_count, joined = query_heads.shape
    head_width = key_heads.shape[-1]
    per_copy = joined // head_width
    block_rows = math.gcd(length, 512)
    blocked = query_heads.reshape(
        length // block_rows, block_rows, item_count, per_copy, head_width
    )

    def one_block(query_block):
        scores = jnp.einsum(
            "qnad,knd->naqk", query_block, key_heads, preferred_element_type=jnp.float32
        ) * head_width ** (-0.5)
        highest = jnp.max(scores, axis=-1, keepdims=True)
        weights = jnp.exp(scores - highest)
        probability = (weights / jnp.sum(weights, axis=-1, keepdims=True)).astype(jnp.bfloat16)
        blended = jnp.einsum(
            "naqk,knd->qnad", probability, value_heads, preferred_element_type=jnp.float32
        )
        return blended.astype(jnp.bfloat16).reshape(block_rows, item_count, joined)

    return lax.map(one_block, blocked).reshape(length, item_count, joined)


def per_device(queries, keys, tokens, w_value, q_gain, k_gain):
    tok_rows = tokens.shape[1]
    devices_sp = lax.axis_size("sp")
    copies = max(devices_sp, KVH)
    repeat_count = copies // KVH
    local_copies = copies // devices_sp
    joined = QH // copies * HD
    token_rows = tokens[0]
    value_sum = jnp.dot(
        token_rows,
        lax.all_gather(w_value, "dp", axis=0, tiled=True),
        preferred_element_type=jnp.float32,
    )
    values = value_sum.astype(jnp.bfloat16).reshape(tok_rows, KVH, HD)
    sp_index = lax.axis_index("sp")
    positions = sp_index * tok_rows + jnp.arange(tok_rows, dtype=jnp.int32)
    row_pos = (positions // GRID_W).astype(jnp.float32)
    col_pos = (positions % GRID_W).astype(jnp.float32)
    query_norm = unit_rms(queries[0].astype(jnp.float32).reshape(tok_rows, QH, HD), q_gain)
    query_rot = rotary(query_norm, row_pos, col_pos).astype(jnp.bfloat16)
    key_norm = unit_rms(keys[0].astype(jnp.float32).reshape(tok_rows, KVH, HD), k_gain)
    key_rot = rotary(key_norm, row_pos, col_pos).astype(jnp.bfloat16)
    query_grouped = query_rot.reshape(tok_rows, copies, joined)
    query_local = lax.all_to_all(query_grouped, "sp", split_axis=1, concat_axis=0, tiled=True)
    key_all, value_all = (
        lax.all_gather(key_rot, "sp", axis=0, tiled=True),
        lax.all_gather(values, "sp", axis=0, tiled=True),
    )
    kv_count = max(1, local_copies // repeat_count)
    kv_start = sp_index * local_copies // repeat_count
    key_local = lax.dynamic_slice_in_dim(key_all, kv_start, kv_count, 1)
    value_local = lax.dynamic_slice_in_dim(value_all, kv_start, kv_count, 1)
    attended = attend(query_local, key_local, value_local)
    returned = lax.all_to_all(attended, "sp", split_axis=0, concat_axis=1, tiled=True)
    return returned.reshape(1, tok_rows, QH * HD)


def solution(mesh):
    in_specs = (
        P("dp", "sp", None),
        P("dp", "sp", None),
        P("dp", "sp", None),
        P("dp", None),
        P(),
        P(),
    )
    out_specs = P("dp", "sp", None)
    return jax.shard_map(
        per_device, mesh=mesh, in_specs=in_specs, out_specs=out_specs, check_vma=False
    )
```

profile of v0, /device:TPU:1, one launch (start us, length us, event | category | flops | bytes accessed | tf_op | source)
XLA Modules:
  0.0 99.3 jit_solution(4973666312808731522)
XLA Ops:
  6.5 0.7 all-gather.2.cloned.1.call-update
  7.3 1.3 %convert_bitcast_fusion = f32[22,8,16,128]{3,1,2,0:T(8,128)S(1)} fusion(bf16[1,176,2048]{2,1,0:T(8,128)(2,1)} %param.8), kind=kLoop, calls=%fused_computation.13 | loop fusion | flops 360448 | bytes 2162688
  8.6 0.3 copy.48
  8.8 0.4 multiply_reduce_fusion
  9.4 0.7 multiply_cosine_fusion.1
  10.1 0.1 copy.36
  10.2 0.4 multiply_multiply_fusion
  10.6 1.2 %subtract_convert_fusion.1 = (bf16[176,16,32]{2,1,0:T(8,128)(2,1)S(1)}, bf16[176,16,32]{2,1,0:T(8,128)(2,1)S(1)}, bf16[176,16,32]{2,1,0:T(8,128)(2,1)S(1)}, bf16[176,16,32]{2,1,0:T(8,128)(2,1)S(1)}) fusion(f32[176,16,128]{2,1,0:T(8,128)S(1)} %multiply_multiply_fusion, f32[176,32]{1,0:T(8,128)S(1)} %get-tuple-element.83, f32[176,32]{1,0:T(8,128)S(1)} %get-tuple-element.82, ...), kind=kLoop, calls=%fused_computation.17 | loop fusion | flops 1441792 | bytes 2252800 | tf_op jit(solution)/shard_map/convert.6
  11.8 0.9 pad_maximum_fusion
  12.8 0.3 convert_element_type.64
  13.1 1.0 copy.37
  14.1 4.4 %all-to-all-start = ((bf16[176,4,512]{2,0,1:T(8,128)(2,1)}), bf16[176,4,512]{2,0,1:T(8,128)(2,1)S(1)}, u32[]{:S(2)}, u32[]{:S(2)}) async-start(bf16[176,4,512]{2,0,1:T(8,128)(2,1)} %copy.37), calls=%async_computation | async-start | bytes 1441792 | tf_op jit(solution)/shard_map/all_to_all | solution.py:96
  18.6 0.3 multiply_reduce_fusion.1
  18.9 0.3 multiply_multiply_fusion.1
  19.1 0.6 subtract_convert_fusion.3
  19.8 0.6 pad_maximum_fusion.1
  20.4 11.6 %all_gather.9 = bf16[704,2,128]{2,1,0:T(2,128)(2,1)S(1)} all-gather(bf16[176,2,128]{2,1,0:T(2,128)(2,1)S(1)} %pad_maximum_fusion.1), channel_id=1, replica_groups=mesh['sp'=4,'dp'=8] {'sp'}, dimensions={0}, use_global_device_ids=true | all-gather | bytes 450560 | tf_op jit(solution)/shard_map/all_gather | solution.py:98
  32.0 0.4 constant_dynamic-slice_fusion.2
  32.4 0.2 reshape.227
  32.6 18.8 %all-gather.2.cloned.1.call-done = bf16[2304,256]{1,0:T(8,128)(2,1)} async-done(((bf16[288,256]{1,0:T(8,128)(2,1)}), bf16[2304,256]{1,0:T(8,128)(2,1)}) %all-gather.2.cloned.1.call-update) | async-done | bytes 1179664 | tf_op jit(solution)/shard_map/all_gather | solution.py:83
  51.4 1.7 %fusion.6 = bf16[22,2,8,128]{3,2,1,0:T(8,128)(2,1)S(1)} fusion(bf16[2304,256]{1,0:T(8,128)(2,1)} %all-gather.2.cloned.1.call-done, bf16[1,176,2304]{2,1,0:T(8,128)(2,1)S(1)} %copy-done), kind=kOutput, calls=%fused_computation.21 | convolution fusion | flops 207663104 | bytes 2080768 | tf_op jit(solution)/shard_map/dot_general | solution.py:81
  53.1 8.0 %all_gather.11 = bf16[704,2,128]{2,0,1:T(8,128)(2,1)S(1)} all-gather(bf16[176,2,128]{2,0,1:T(8,128)(2,1)S(1)} %bitcast.73), channel_id=1, replica_groups=mesh['sp'=4,'dp'=8] {'sp'}, dimensions={0}, use_global_device_ids=true | all-gather | bytes 450560 | tf_op jit(solution)/shard_map/all_gather | solution.py:99
  61.1 13.4 %while.10 = (s32[]{:T(128)}, bf16[11,64,1,512]{3,1,2,0:T(8,128)(2,1)S(1)}, bf16[11,64,1,4,128]{4,3,1,0,2:T(4,128)(2,1)S(1)}, bf16[704,1,128]{2,0,1:T(8,128)(2,1)...) while((s32[]{:T(128)}, bf16[11,64,1,512]{3,1,2,0:T(8,128)(2,1)S(1)}, ...), condition=%wide.region_5.6_spmd, body=%wide.region_2.5_spmd.sunk | while | flops 93568512 | bytes 3183693 | solution.py:70
  61.2 0.4 fusion.20
  61.6 0.3 fusion.21
  61.8 0.4 fusion.22
  62.4 0.4 fusion.20
  62.8 0.3 fusion.21
  63.1 0.4 fusion.22
  63.6 0.4 fusion.20
  64.0 0.3 fusion.21
  64.3 0.4 fusion.22
  64.9 0.4 fusion.20
  65.2 0.3 fusion.21
  65.5 0.4 fusion.22
  66.1 0.4 fusion.20
  66.4 0.3 fusion.21
  66.7 0.4 fusion.22
  67.3 0.4 fusion.20
  67.7 0.3 fusion.21
  67.9 0.4 fusion.22
  68.5 0.4 fusion.20
  68.9 0.3 fusion.21
  69.2 0.4 fusion.22
  69.7 0.4 fusion.20
  70.1 0.3 fusion.21
  70.4 0.4 fusion.22
  71.0 0.4 fusion.20
  71.3 0.3 fusion.21
  71.6 0.4 fusion.22
  72.2 0.4 fusion.20
  72.5 0.3 fusion.21
  72.8 0.4 fusion.22
  73.4 0.4 fusion.20
  73.8 0.3 fusion.21
  74.0 0.4 fusion.22
  74.6 0.5 broadcast.195
  75.1 1.2 %reduce.2 = bf16[704,512]{1,0:T(8,128)(2,1)S(1)} reduce(bf16[704,1,512]{2,0,1:T(8,128)(2,1)S(1)} %bitcast.72, bf16[]{:T(256)} %broadcast.195), dimensions={1}, to_apply=%copy.43.reduce_sub_computation | reduce | bytes 1441794 | tf_op jit(solution)/shard_map/reshape | solution.py:70
  76.3 0.6 reshape.235
  76.9 12.7 %all_to_all.30 = bf16[4,2,45056]{2,1,0:T(2,128)(2,1)S(1)} all-to-all(bf16[4,2,45056]{2,1,0:T(2,128)(2,1)S(1)} %reshape.235), channel_id=1, replica_groups=mesh['sp'=4,'dp'=8] {'sp'}, dimensions={0} | all-to-all | bytes 1441792 | tf_op jit(solution)/shard_map/all_to_all | solution.py:106
  89.6 0.7 reshape.236
  90.3 0.2 copy.46
  90.5 0.6 copy.44
  91.1 1.4 %reshape.230 = bf16[1,176,2048]{2,1,0:T(8,128)(2,1)} reshape(bf16[176,4,1,512]{3,1,0,2:T(4,128)(2,1)S(1)} %copy.44) | data formatting | bytes 1441792 | tf_op jit(solution)/shard_map/reshape | solution.py:107
  (64 shorter events, 1.7 us)
Async XLA Ops:
  6.5 44.9 %copy-start = (bf16[1,176,2304]{2,1,0:T(8,128)(2,1)S(1)}, bf16[1,176,2304]{2,1,0:T(8,128)(2,1)}, u32[]{:S(2)}) copy-start(bf16[1,176,2304]{2,1,0:T(8,128)(2,1)} %param.10) | copy-start | bytes 2433028
  6.5 44.9 %all-gather.2.cloned.1.call-start = ((), (), s32[]{:S(2)}) async-start(), calls=%async_computation.2 | async-start | bytes 1327104 | tf_op jit(solution)/shard_map/all_gather | solution.py:83
  8.8 1.4 %copy-start.2 = (f32[128]{0:T(128)S(1)}, f32[128]{0:T(128)}, u32[]{:S(2)}) copy-start(f32[128]{0:T(128)} %param.12) | copy-start | bytes 1540
  13.1 5.4 %copy-start.1 = (bf16[1,176,256]{2,1,0:T(8,128)(2,1)S(1)}, bf16[1,176,256]{2,1,0:T(8,128)(2,1)}, u32[]{:S(2)}) copy-start(bf16[1,176,256]{2,1,0:T(8,128)(2,1)} %param.9) | copy-start | bytes 270340
  14.1 4.8 %copy-start.3 = (f32[128]{0:T(128)S(1)}, f32[128]{0:T(128)}, u32[]{:S(2)}) copy-start(f32[128]{0:T(128)} %param.13) | copy-start | bytes 1540
  14.1 18.4 %all-to-all-start = ((bf16[176,4,512]{2,0,1:T(8,128)(2,1)}), bf16[176,4,512]{2,0,1:T(8,128)(2,1)S(1)}, u32[]{:S(2)}, u32[]{:S(2)}) async-start(bf16[176,4,512]{2,0,1:T(8,128)(2,1)} %copy.37), calls=%async_computation | async-start | bytes 1441792 | tf_op jit(solution)/shard_map/all_to_all | solution.py:96
Sparse Core Ops, SparseCore 0:
  9.5 41.8 all-gather.1
where the time goes:
time: 100 us; the launch traced here: 99.3 us
  blocking collectives  32.4 us (32%)
  waiting for transfers between devices  19.6 us (20%)
  between operations  13.6 us (14%)
  other arithmetic  11 us (11%)
  matrix products  10 us (10%)
  local copies, waits for them, and re-layouts  7.71 us (8%)
  starting transfers between devices  4.41 us (4%)
    all_gather x1, waiting for transfers between devices, per_device(): lax.all_gather(w_value, 'dp', axis=0, tiled=True)  18.8 us
    all_to_all x1, blocking collectives, per_device(): lax.all_to_all(attended, 'sp', split_axis=0, concat_axis=1, tiled=True)  12.7 us
    all_gather x1, blocking collectives, per_device(): lax.all_gather(key_rot, 'sp', axis=0, tiled=True)  11.6 us
    all_gather x1, blocking collectives, per_device(): lax.all_gather(values, 'sp', axis=0, tiled=True)  8.01 us
    all_to_all x1, starting transfers between devices, per_device(): lax.all_to_all(query_grouped, 'sp', split_axis=1, concat_axis=0, tiled=True)  4.41 us
    dot_general x11, matrix products, one_block(): jnp.einsum('naqk,knd->qnad', probability, value_heads, preferred_element_...  4.41 us
    dot_general x11, matrix products, one_block(): jnp.einsum('qnad,knd->naqk', query_block, key_heads, preferred_element_ty...  3.98 us
    reduce_sum x11, other arithmetic, one_block(): jnp.sum(weights, axis=-1, keepdims=True)  3.07 us
  transfers between devices with their start and end apart: 2, of which 1 were waited for; matrix products, arithmetic and copies ran while one was open for 9% of the time, Pallas kernels for 0%

commit v1 on v0

v1 whole, which is shorter than its diff:
```python
import functools
import math

import jax
import jax.numpy as jnp
import numpy as np
from jax import lax
from jax.experimental import pallas as pl
from jax.experimental.pallas import tpu as pltpu
from jax.sharding import PartitionSpec as P

HD = 128
QH = 16
KVH = 2
GRID_W = 64
GROUP = QH // KVH
epsilon = 1e-06
MESH = pl.DeviceIdType.MESH


def inner_size(n):
    size = 1
    while size * size * 4 <= n and n % (size * 2) == 0:
        size *= 2
    return size


def kernel(
    n_sp, n_dp, q_hbm, k_hbm, tok_hbm, w_hbm, qg_ref, kg_ref, freq_ref, out_hbm,
    q_in, k_in, tok, w_in, wbuf, kbuf, vbuf, qrot, prob, outbuf, cos_ref, sin_ref,
    in_sem, w_z, w_x, w_s, w_recv, w_srecv, k_send, k_recv, v_send, v_recv, v_fwd, v_frecv, out_sem,
):
    rows = q_hbm.shape[0]
    depth = w_hbm.shape[0]
    n_x = inner_size(n_dp)
    n_z = n_dp // n_x
    n_y = n_sp // 2
    sp = lax.axis_index("sp")
    dp = lax.axis_index("dp")
    z, x = dp // n_x, dp % n_x
    y, c = sp // 2, sp % 2
    sib = y * 2 + (1 - c)

    loads = [
        pltpu.make_async_copy(src, dst, in_sem.at[i])
        for i, (src, dst) in enumerate(
            ((w_hbm, w_in), (k_hbm, k_in), (q_hbm, q_in), (tok_hbm, tok))
        )
    ]
    for load in loads:
        load.start()

    z_peers = [((z + d) % n_z) for d in range(1, n_z)]
    x_peers = [((x + d) % n_x) for d in range(1, n_x)]
    sp_peers = [((sp + d) % n_sp) for d in range(1, n_sp)]
    y_peers = [((y + d) % n_y) for d in range(1, n_y)]

    barrier = pltpu.get_barrier_semaphore()
    for zp in z_peers:
        pl.semaphore_signal(barrier, inc=1, device_id=(sp, zp * n_x + x), device_id_type=MESH)
    for xp in x_peers:
        pl.semaphore_signal(barrier, inc=1, device_id=(sp, z * n_x + xp), device_id_type=MESH)
    for j in sp_peers:
        pl.semaphore_signal(barrier, inc=1, device_id=(j, dp), device_id_type=MESH)
    pl.semaphore_wait(barrier, n_z - 1 + n_x - 1 + n_sp - 1)

    pending = []

    def remote(src, dst, send, recv, where):
        return pltpu.make_async_remote_copy(
            src_ref=src, dst_ref=dst, send_sem=send, recv_sem=recv, device_id=where, device_id_type=MESH
        )

    def send(*args):
        copy = remote(*args)
        copy.start()
        pending.append(copy)

    def block(d, core):
        return wbuf.at[pl.ds(pl.multiple_of(d * depth, 16), depth), pl.ds(pl.multiple_of(core * HD, HD), HD)]

    mine = w_in.at[:, pl.ds(pl.multiple_of(c * HD, HD), HD)]
    loads[0].wait()
    for i, zp in enumerate(z_peers):
        send(mine, block(dp, c), w_z.at[i], w_recv.at[dp], (sp, zp * n_x + x))
    for i, xp in enumerate(x_peers):
        send(mine, block(dp, c), w_x.at[0, i], w_recv.at[dp], (sp, z * n_x + xp))

    pos = sp * rows + lax.broadcasted_iota(jnp.int32, (rows, HD), 0)
    lane = lax.broadcasted_iota(jnp.int32, (rows, HD), 1)
    grid_row = pos // GRID_W
    coord = jnp.where(lane < HD // 2, grid_row, pos - grid_row * GRID_W).astype(jnp.float32)
    angles = coord * freq_ref[...]
    first = lane % (HD // 2) < HD // 4
    cos_ref[...] = jnp.cos(angles)
    sine = jnp.sin(angles)
    sin_ref[...] = jnp.where(first, -sine, sine)

    def norm_rot(u, gain):
        u = u.astype(jnp.float32)
        u = u * lax.rsqrt(jnp.mean(u * u, axis=-1, keepdims=True) + epsilon) * gain
        other = jnp.where(first, pltpu.roll(u, HD - HD // 4, 1), pltpu.roll(u, HD // 4, 1))
        return (u * cos_ref[...] + other * sin_ref[...]).astype(jnp.bfloat16)

    def at(ref, s):
        return ref.at[pl.ds(pl.multiple_of(s * rows, 16), rows), :]

    own = pl.ds(pl.multiple_of(sp * rows, 16), rows)
    loads[1].wait()
    for g in range(KVH):
        kbuf[own, g * HD:(g + 1) * HD] = norm_rot(k_in[:, g * HD:(g + 1) * HD], kg_ref[...])
    for i, j in enumerate(sp_peers):
        send(at(kbuf, sp), at(kbuf, sp), k_send.at[i], k_recv.at[sp], (j, dp))

    wbuf[pl.ds(pl.multiple_of(dp * depth, 16), depth), :] = w_in[...]
    loads[2].wait()
    for h in range(QH):
        qrot[h] = norm_rot(q_in[:, h * HD:(h + 1) * HD], qg_ref[...])

    for j in sp_peers:
        remote(at(kbuf, j), at(kbuf, j), k_send.at[0], k_recv.at[j], (j, dp)).wait_recv()

    scale = HD ** -0.5 * math.log2(math.e)

    def weights(h, g):
        s = lax.dot_general(
            qrot[h], kbuf[:, g * HD:(g + 1) * HD], (((1,), (1,)), ((), ())),
            preferred_element_type=jnp.float32,
        )
        e = jnp.exp2((s - jnp.max(s, axis=-1, keepdims=True)) * scale)
        prob[h] = (e * (1.0 / jnp.sum(e, axis=-1, keepdims=True))).astype(jnp.bfloat16)

    def relay_z(i):
        d = z_peers[i] * n_x + x
        remote(block(d, c), block(d, c), w_z.at[0], w_recv.at[d], (sp, d)).wait_recv()
        for k, xp in enumerate(x_peers):
            send(block(d, c), block(d, c), w_x.at[i + 1, k], w_recv.at[d], (sp, z * n_x + xp))
        send(block(d, c), block(d, c), w_s.at[d], w_srecv.at[d], (sib, dp))

    def relay_x(zi, k):
        zz = z if zi < 0 else z_peers[zi]
        d = zz * n_x + x_peers[k]
        remote(block(d, c), block(d, c), w_z.at[0], w_recv.at[d], (sp, d)).wait_recv()
        send(block(d, c), block(d, c), w_s.at[d], w_srecv.at[d], (sib, dp))

    order = sorted(range(n_z - 1), key=lambda i: min(i + 1, n_z - 1 - i))
    relays = [functools.partial(relay_x, -1, k) for k in range(n_x - 1)]
    relays += [functools.partial(relay_z, i) for i in order]
    relays += [functools.partial(relay_x, i, k) for i in order for k in range(n_x - 1)]
    done = 0
    for part in range(GROUP // 2):
        count = len(relays) * (part + 1) // (GROUP // 2)
        for relay in relays[done:count]:
            relay()
        done = count
        for g in range(KVH):
            base = g * GROUP + part * 2

            @pl.loop(base, base + 2)
            def _(h, g=g):
                weights(h, g)

    for d in [z * n_x + xp for xp in x_peers] + [
        zp * n_x + xx for zp in z_peers for xx in [x] + x_peers
    ]:
        theirs = block(d, 1 - c)
        remote(theirs, theirs, w_s.at[0], w_srecv.at[d], (sib, dp)).wait_recv()

    loads[3].wait()
    vbuf[own, :] = jnp.dot(tok[...], wbuf[...], preferred_element_type=jnp.float32).astype(jnp.bfloat16)
    for i, yp in enumerate(y_peers):
        send(at(vbuf, sp), at(vbuf, sp), v_send.at[i], v_recv.at[sp], (yp * 2 + c, dp))
    send(at(vbuf, sp), at(vbuf, sp), v_send.at[n_y - 1], v_recv.at[sp], (sib, dp))
    for i, yp in enumerate(y_peers):
        j = yp * 2 + c
        remote(at(vbuf, j), at(vbuf, j), v_send.at[0], v_recv.at[j], (j, dp)).wait_recv()
        send(at(vbuf, j), at(vbuf, j), v_fwd.at[i], v_frecv.at[j], (sib, dp))
    remote(at(vbuf, sib), at(vbuf, sib), v_send.at[0], v_recv.at[sib], (sib, dp)).wait_recv()
    for yp in y_peers:
        j = yp * 2 + 1 - c
        remote(at(vbuf, j), at(vbuf, j), v_send.at[0], v_frecv.at[j], (sib, dp)).wait_recv()

    stores = []
    for part in range(4):
        for h in range(part * QH // 4, (part + 1) * QH // 4):
            g = h // GROUP
            outbuf[:, h * HD:(h + 1) * HD] = jnp.dot(
                prob[h], vbuf[:, g * HD:(g + 1) * HD], preferred_element_type=jnp.float32
            ).astype(jnp.bfloat16)
        cols = pl.ds(part * QH // 4 * HD, QH // 4 * HD)
        stores.append(pltpu.make_async_copy(outbuf.at[:, cols], out_hbm.at[:, cols], out_sem.at[part]))
        stores[-1].start()
    for copy in pending:
        copy.wait_send()
    for store in stores:
        store.wait()


def per_device(queries, keys, tokens, w_value, q_gain, k_gain):
    n_sp, n_dp = lax.axis_size("sp"), lax.axis_size("dp")
    n_x = inner_size(n_dp)
    n_z = n_dp // n_x
    n_y = n_sp // 2
    rows, width = tokens.shape[1:]
    depth = w_value.shape[0]
    quarter = HD // 4
    freq = 10000.0 ** (-jnp.arange(quarter, dtype=jnp.float32) * 2.0 / (HD // 2))
    freq = jnp.tile(freq, 4)[None]
    any_spec = pl.BlockSpec(memory_space=pl.ANY)
    vmem = pl.BlockSpec(memory_space=pltpu.VMEM)
    bf16 = jnp.bfloat16
    dma = pltpu.SemaphoreType.DMA
    out = pl.pallas_call(
        functools.partial(kernel, n_sp, n_dp),
        out_shape=jax.ShapeDtypeStruct((rows, QH * HD), bf16),
        in_specs=[any_spec] * 4 + [vmem] * 3,
        out_specs=any_spec,
        scratch_shapes=[
            pltpu.VMEM((rows, QH * HD), bf16),
            pltpu.VMEM((rows, KVH * HD), bf16),
            pltpu.VMEM((rows, width), bf16),
            pltpu.VMEM((depth, KVH * HD), bf16),
            pltpu.VMEM((width, KVH * HD), bf16),
            pltpu.VMEM((rows * n_sp, KVH * HD), bf16),
            pltpu.VMEM((rows * n_sp, KVH * HD), bf16),
            pltpu.VMEM((QH, rows, HD), bf16),
            pltpu.VMEM((QH, rows, rows * n_sp), bf16),
            pltpu.VMEM((rows, QH * HD), bf16),
            pltpu.VMEM((rows, HD), jnp.float32),
            pltpu.VMEM((rows, HD), jnp.float32),
            dma((4,)),
            dma((n_z,)),
            dma((n_z, n_x)),
            dma((n_dp,)),
            dma((n_dp,)),
            dma((n_dp,)),
            dma((n_sp,)),
            dma((n_sp,)),
            dma((n_y,)),
            dma((n_sp,)),
            dma((n_y,)),
            dma((n_sp,)),
            dma((4,)),
        ],
        compiler_params=pltpu.CompilerParams(
            collective_id=0, has_side_effects=True, vmem_limit_bytes=60 * 1024 * 1024
        ),
        name="fused_attention",
    )(queries[0], keys[0], tokens[0], w_value, q_gain[None], k_gain[None], freq)
    return out[None]


def solution(mesh):
    in_specs = (
        P("dp", "sp", None),
        P("dp", "sp", None),
        P("dp", "sp", None),
        P("dp", None),
        P(),
        P(),
    )
    return jax.shard_map(
        per_device, mesh=mesh, in_specs=in_specs, out_specs=P("dp", "sp", None), check_vma=False
    )
```

time: 100 us -> 32.8 us (0.33)
  blocking collectives: 32.4 us -> 0 us
  Pallas kernels: 0 us -> 30 us
  waiting for transfers between devices: 19.6 us -> 0 us
  between operations: 13.6 us -> 0.01 us
  other arithmetic: 11 us -> 0.01 us
  matrix products: 10 us -> 0 us
  local copies, waits for them, and re-layouts: 7.71 us -> 2.64 us
  starting transfers between devices: 4.41 us -> 0 us
    pallas_call x0 -> x1, Pallas kernels: none -> 30 us  [per_device(): pl.pallas_call(functools.partial(kernel, n_sp, n_dp), out_shape=jax.Shape...]
    all_gather x2 -> x0, blocking collectives: 19.7 us -> none  [the longest x1 11.6 us: per_device(): lax.all_gather(key_rot, 'sp', axis=0, tiled=True)]
    all_gather x1 -> x0, waiting for transfers between devices: 18.8 us -> none  [per_device(): lax.all_gather(w_value, 'dp', axis=0, tiled=True)]
    all_to_all x1 -> x0, blocking collectives: 12.7 us -> none  [per_device(): lax.all_to_all(attended, 'sp', split_axis=0, concat_axis=1, tiled=True)]
    dot_general x23 -> x0, matrix products: 10 us -> none  [the longest x11 4.41 us: one_block(): jnp.einsum('naqk,knd->qnad', probability, value_heads, preferred_element_...]
    all_to_all x1 -> x0, starting transfers between devices: 4.41 us -> none  [per_device(): lax.all_to_all(query_grouped, 'sp', split_axis=1, concat_axis=0, tiled=True)]
    reduce_sum x13 -> x0, other arithmetic: 3.77 us -> none  [the longest x11 3.07 us: one_block(): jnp.sum(weights, axis=-1, keepdims=True)]
    reshape x4 -> x0, local copies, waits for them, and re-layouts: 2.08 us -> none  [the longest x1 1.39 us: per_device(): return returned.reshape(1, tok_rows, QH * HD)]
  transfers between devices with their start and end apart: 2 -> 0, of which waited for: 1 -> 0; matrix products, arithmetic and copies ran while one was open for 9% -> 0% of each run, Pallas kernels for 0% -> 0%
where the time goes in v1:
time: 32.8 us; the launch traced here: 32.7 us
  Pallas kernels  30 us (91%)
  local copies, waits for them, and re-layouts  2.64 us (8%)
    pallas_call x1, Pallas kernels, per_device(): pl.pallas_call(functools.partial(kernel, n_sp, n_dp), out_shape=jax.Shape...  30 us
    unnamed x1, local copies, waits for them, and re-layouts  2.04 us

profile of v1, /device:TPU:1, one launch (start us, length us, event | category | flops | bytes accessed | tf_op | source)
XLA Modules:
  0.0 32.7 jit_solution(14514635058837137172)
XLA Ops:
  0.0 0.6 %broadcast_in_dim_tile.3.freq_ref = f32[1,128]{1,0:T(1,128)} reshape(f32[4,32]{1,0:T(4,128)S(1)} %tile.2) | data formatting | bytes 1024 | tf_op jit(solution)/shard_map/broadcast_in_dim;tile | solution.py:208
  0.6 30.0 %fused_attention.1 = bf16[176,2048]{1,0:T(8,128)(2,1)} custom-call(bf16[176,2048]{1,0:T(8,128)(2,1)} %bitcast.8, bf16[176,256]{1,0:T(8,128)(2,1)} %bitcast.9, bf16[176,2304]{1,0:T(8,128)(2,1)} %bitcast.7, bf16[288,256]{1,0:T(8,128)(2,1)} %w_hbm.1, f32[1,128]{1,0:T(1,128)} %bitcast.10, f32[1,128]{1,0:T(1,128)} %bitcast.11, f32[1,128]{1,0:T(1,128)} %broadcast_in_dim_tile.3.freq_ref), custom_call_target="tpu_custom_call" | custom-call | tf_op jit(solution)/shard_map/fused_attention/pallas_call | solution.py:213
  30.6 2.0 %copy.8 = bf16[1,176,2048]{2,1,0:T(8,128)(2,1)} copy(bf16[1,176,2048]{2,1,0:T(8,128)(2,1)} %bitcast.6) | data formatting | bytes 1441792
  (2 shorter events, 0.0 us)

commit v2 on v1

v2 whole, which is shorter than its diff:
```python
import functools
import math

import jax
import jax.numpy as jnp
from jax import lax
from jax.experimental import pallas as pl
from jax.experimental.pallas import tpu as pltpu
from jax.sharding import PartitionSpec as P

HD = 128
QH = 16
KVH = 2
GRID_W = 64
GROUP = QH // KVH
epsilon = 1e-06
MESH = pl.DeviceIdType.MESH


def inner_size(n):
    size = 1
    while size * size * 4 <= n and n % (size * 2) == 0:
        size *= 2
    return size


def kernel(
    n_sp, n_dp, q_hbm, k_hbm, tok_hbm, w_hbm, qg_hbm, kg_hbm, out_ref,
    q_in, k_in, tok, wbuf, kbuf, vbuf, qrot, prob, cos_ref, sin_ref, qg_ref, kg_ref,
    in_sem, w_z, w_x, w_recv, t_send, t_recv, k_send, k_recv, k_fwd, k_frecv, v_send, v_recv, v_fwd, v_frecv,
):
    rows = q_hbm.shape[0]
    depth = w_hbm.shape[0]
    n_x = inner_size(n_dp)
    n_z = n_dp // n_x
    n_y = n_sp // 2
    sp = lax.axis_index("sp")
    dp = lax.axis_index("dp")
    z, x = dp // n_x, dp % n_x
    y, c = sp // 2, sp % 2
    sib = y * 2 + (1 - c)

    def block(d):
        return wbuf.at[pl.ds(pl.multiple_of(d * depth, 16), depth), :]

    def token_part(core):
        return tok.at[pl.ds(pl.multiple_of(core * rows, 16), rows), :]

    z_peers = [((z + d) % n_z) for d in range(1, n_z)]
    x_peers = [((x + d) % n_x) for d in range(1, n_x)]
    y_peers = [((y + d) % n_y) for d in range(1, n_y)]

    barrier = pltpu.get_barrier_semaphore()
    for zp in z_peers:
        pl.semaphore_signal(barrier, inc=1, device_id=(sp, zp * n_x + x), device_id_type=MESH)
    for xp in x_peers:
        pl.semaphore_signal(barrier, inc=1, device_id=(sp, z * n_x + xp), device_id_type=MESH)
    for yp in y_peers:
        pl.semaphore_signal(barrier, inc=1, device_id=(yp * 2 + c, dp), device_id_type=MESH)
    pl.semaphore_signal(barrier, inc=1, device_id=(sib, dp), device_id_type=MESH)

    w_mine = w_hbm.at[:, pl.ds(pl.multiple_of(c * HD, HD), HD)]
    loads = [
        pltpu.make_async_copy(src, dst, in_sem.at[i])
        for i, (src, dst) in enumerate(
            (
                (kg_hbm, kg_ref), (k_hbm, k_in), (w_mine, block(dp)), (tok_hbm, token_part(c)),
                (q_hbm, q_in), (qg_hbm, qg_ref),
            )
        )
    ]
    for load in loads:
        load.start()

    pending = []

    def remote(src, dst, send, recv, where):
        return pltpu.make_async_remote_copy(
            src_ref=src, dst_ref=dst, send_sem=send, recv_sem=recv, device_id=where, device_id_type=MESH
        )

    def send(*args):
        copy = remote(*args)
        copy.start()
        pending.append(copy)

    pos = sp * rows + lax.broadcasted_iota(jnp.int32, (rows, HD), 0)
    lane = lax.broadcasted_iota(jnp.int32, (rows, HD), 1)
    grid_row = pos // GRID_W
    coord = jnp.where(lane < HD // 2, grid_row, pos - grid_row * GRID_W).astype(jnp.float32)
    step = (lax.broadcasted_iota(jnp.int32, (1, HD), 1) % (HD // 4)).astype(jnp.float32)
    angles = coord * jnp.exp2(step * (-2.0 * math.log2(10000.0) / (HD // 2)))
    first = lane % (HD // 2) < HD // 4
    cos_ref[...] = jnp.cos(angles)
    sine = jnp.sin(angles)
    sin_ref[...] = jnp.where(first, -sine, sine)

    def norm_rot(u, gain):
        u = u.astype(jnp.float32)
        u = u * lax.rsqrt(jnp.mean(u * u, axis=-1, keepdims=True) + epsilon) * gain
        other = jnp.where(first, pltpu.roll(u, HD - HD // 4, 1), pltpu.roll(u, HD // 4, 1))
        return (u * cos_ref[...] + other * sin_ref[...]).astype(jnp.bfloat16)

    def at(ref, s):
        return ref.at[pl.ds(pl.multiple_of(s * rows, 16), rows), :]

    own = pl.ds(pl.multiple_of(sp * rows, 16), rows)
    loads[0].wait()
    loads[1].wait()
    for g in range(KVH):
        kbuf[own, g * HD:(g + 1) * HD] = norm_rot(k_in[:, g * HD:(g + 1) * HD], kg_ref[...])
    loads[2].wait()

    pl.semaphore_wait(barrier, n_z - 1 + n_x - 1 + n_y)
    for i, zp in enumerate(z_peers):
        send(block(dp), block(dp), w_z.at[i], w_recv.at[dp], (sp, zp * n_x + x))
    for i, xp in enumerate(x_peers):
        send(block(dp), block(dp), w_x.at[0, i], w_recv.at[dp], (sp, z * n_x + xp))
    for i, yp in enumerate(y_peers):
        send(at(kbuf, sp), at(kbuf, sp), k_send.at[i], k_recv.at[y], (yp * 2 + c, dp))
    send(at(kbuf, sp), at(kbuf, sp), k_send.at[n_y - 1], k_frecv.at[y], (sib, dp))
    loads[3].wait()
    send(token_part(c), token_part(c), t_send.at[0], t_recv.at[0], (sib, dp))

    loads[4].wait()
    loads[5].wait()
    for h in range(QH):
        qrot[h] = norm_rot(q_in[:, h * HD:(h + 1) * HD], qg_ref[...])

    for i, yp in enumerate(y_peers):
        j = yp * 2 + c
        remote(at(kbuf, j), at(kbuf, j), k_send.at[0], k_recv.at[yp], (j, dp)).wait_recv()
        send(at(kbuf, j), at(kbuf, j), k_fwd.at[i], k_frecv.at[yp], (sib, dp))
    for yp in [y] + y_peers:
        j = yp * 2 + 1 - c
        remote(at(kbuf, j), at(kbuf, j), k_send.at[0], k_frecv.at[yp], (sib, dp)).wait_recv()

    scale = HD ** -0.5 * math.log2(math.e)

    def weights(h, g):
        s = lax.dot_general(
            qrot[h], kbuf[:, g * HD:(g + 1) * HD], (((1,), (1,)), ((), ())),
            preferred_element_type=jnp.float32,
        )
        e = jnp.exp2((s - jnp.max(s, axis=-1, keepdims=True)) * scale)
        prob[h] = (e * (1.0 / jnp.sum(e, axis=-1, keepdims=True))).astype(jnp.bfloat16)

    def arrived(d):
        remote(block(d), block(d), w_z.at[0], w_recv.at[d], (sp, d)).wait_recv()

    def relay(i):
        d = z_peers[i] * n_x + x
        arrived(d)
        for k, xp in enumerate(x_peers):
            send(block(d), block(d), w_x.at[i + 1, k], w_recv.at[d], (sp, z * n_x + xp))

    order = sorted(range(n_z - 1), key=lambda i: min(i + 1, n_z - 1 - i))
    relays = [functools.partial(relay, i) for i in order]
    done = 0
    for part in range(GROUP // 2):
        count = len(relays) * (part + 1) // (GROUP // 2)
        for step_on in relays[done:count]:
            step_on()
        done = count
        for g in range(KVH):
            base = g * GROUP + part * 2

            @pl.loop(base, base + 2)
            def _(h, g=g):
                weights(h, g)

    for zz in [z] + [z_peers[i] for i in order]:
        for xp in x_peers:
            arrived(zz * n_x + xp)
    theirs = token_part(1 - c)
    remote(theirs, theirs, t_send.at[0], t_recv.at[0], (sib, dp)).wait_recv()

    def chip(head, yy):
        return vbuf.at[head, pl.ds(pl.multiple_of(yy * 2 * rows, 16), 2 * rows), :]

    chip(c, y)[...] = jnp.dot(tok[...], wbuf[...], preferred_element_type=jnp.float32).astype(jnp.bfloat16)
    for i, yp in enumerate(y_peers):
        send(chip(c, y), chip(c, y), v_send.at[i], v_recv.at[y], (yp * 2 + c, dp))
    send(chip(c, y), chip(c, y), v_send.at[n_y - 1], v_frecv.at[y], (sib, dp))
    for i, yp in enumerate(y_peers):
        there = chip(c, yp)
        remote(there, there, v_send.at[0], v_recv.at[yp], (yp * 2 + c, dp)).wait_recv()
        send(there, there, v_fwd.at[i], v_frecv.at[yp], (sib, dp))
    for yp in [y] + y_peers:
        there = chip(1 - c, yp)
        remote(there, there, v_send.at[0], v_frecv.at[yp], (sib, dp)).wait_recv()

    for h in range(QH):
        out_ref[:, h * HD:(h + 1) * HD] = jnp.dot(
            prob[h], vbuf[h // GROUP], preferred_element_type=jnp.float32
        ).astype(jnp.bfloat16)
    for copy in pending:
        copy.wait_send()


def per_device(queries, keys, tokens, w_value, q_gain, k_gain):
    n_sp, n_dp = lax.axis_size("sp"), lax.axis_size("dp")
    n_x = inner_size(n_dp)
    n_z = n_dp // n_x
    n_y = n_sp // 2
    rows, width = tokens.shape[1:]
    depth = w_value.shape[0]
    any_spec = pl.BlockSpec(memory_space=pltpu.HBM)
    bf16, f32 = jnp.bfloat16, jnp.float32
    dma = pltpu.SemaphoreType.DMA
    length = rows * n_sp
    buffers = [
        ((rows, QH * HD), bf16),
        ((rows, KVH * HD), bf16),
        ((2 * rows, width), bf16),
        ((width, HD), bf16),
        ((length, KVH * HD), bf16),
        ((KVH, length, HD), bf16),
        ((QH, rows, HD), bf16),
        ((QH, rows, length), bf16),
        ((rows, HD), f32),
        ((rows, HD), f32),
        ((1, HD), f32),
        ((1, HD), f32),
    ]
    held = sum(math.prod(shape) * jnp.dtype(kind).itemsize for shape, kind in buffers)
    limit = min(60 * 2 ** 20, held + held // 4 + 8 * rows * length * 4 + 4 * 2 ** 20)
    out = pl.pallas_call(
        functools.partial(kernel, n_sp, n_dp),
        out_shape=jax.ShapeDtypeStruct((rows, QH * HD), bf16),
        in_specs=[any_spec] * 6,
        out_specs=pl.BlockSpec(memory_space=pltpu.VMEM),
        scratch_shapes=[pltpu.VMEM(shape, kind) for shape, kind in buffers]
        + [
            dma((6,)),
            dma((n_z,)),
            dma((n_z, n_x)),
            dma((n_dp,)),
            dma((1,)),
            dma((1,)),
            dma((n_y,)),
            dma((n_y,)),
            dma((n_y,)),
            dma((n_y,)),
            dma((n_y,)),
            dma((n_y,)),
            dma((n_y,)),
            dma((n_y,)),
        ],
        compiler_params=pltpu.CompilerParams(
            collective_id=0, has_side_effects=True, vmem_limit_bytes=limit
        ),
        name="fused_attention",
    )(queries[0], keys[0], tokens[0], w_value, q_gain[None], k_gain[None])
    return out[None]


def solution(mesh):
    in_specs = (
        P("dp", "sp", None),
        P("dp", "sp", None),
        P("dp", "sp", None),
        P("dp", None),
        P(),
        P(),
    )
    return jax.shard_map(
        per_device, mesh=mesh, in_specs=in_specs, out_specs=P("dp", "sp", None), check_vma=False
    )
```

time: 32.8 us -> 32.3 us (0.985)
  Pallas kernels: 30 us -> 26.5 us
  local copies, waits for them, and re-layouts: 2.64 us -> 5.58 us
    pallas_call x1, Pallas kernels: 30 us -> 26.5 us  [per_device(): pl.pallas_call(functools.partial(kernel, n_sp, n_dp), out_shape=jax.Shape...]
    unnamed x1 -> x13, local copies, waits for them, and re-layouts: 2.04 us -> 5.58 us
    another operation x2 -> x0, local copies, waits for them, and re-layouts: 0.6 us -> none  [per_device(): freq = jnp.tile(freq, 4)[None]]
where the time goes in v2:
time: 32.3 us; the launch traced here: 32.1 us
  Pallas kernels  26.5 us (82%)
  local copies, waits for them, and re-layouts  5.58 us (17%)
    pallas_call x1, Pallas kernels, per_device(): pl.pallas_call(functools.partial(kernel, n_sp, n_dp), out_shape=jax.Shape...  26.5 us
    unnamed x13, local copies, waits for them, and re-layouts  5.58 us

profile of v2, /device:TPU:1, one launch (start us, length us, event | category | flops | bytes accessed | tf_op | source)
XLA Modules:
  0.0 32.1 jit_solution(13651429068925297634)
XLA Ops:
  0.0 0.0 copy-start.4
  0.0 0.0 copy-start.5
  0.0 0.7 %copy-done.4 = f32[128]{0:T(128)S(1)} copy-done((f32[128]{0:T(128)S(1)}, f32[128]{0:T(128)}, u32[]{:S(2)}) %copy-start.4) | copy-done | bytes 536
  0.7 0.0 copy-done.5
  0.7 0.0 copy-start
  0.7 1.1 %copy-done = bf16[1,176,2304]{2,1,0:T(8,128)(2,1)S(1)} copy-done((bf16[1,176,2304]{2,1,0:T(8,128)(2,1)S(1)}, bf16[1,176,2304]{2,1,0:T(8,128)(2,1)}, u32[]{:S(2)}) %copy-start) | copy-done | bytes 811032
  1.8 0.0 copy-start.1
  1.8 1.1 %copy-done.1 = bf16[1,176,2048]{2,1,0:T(8,128)(2,1)S(1)} copy-done((bf16[1,176,2048]{2,1,0:T(8,128)(2,1)S(1)}, bf16[1,176,2048]{2,1,0:T(8,128)(2,1)}, u32[]{:S(2)}) %copy-start.1) | copy-done | bytes 720920
  2.9 0.0 copy-start.2
  2.9 0.9 %copy-done.2 = bf16[288,256]{1,0:T(8,128)(2,1)S(1)} copy-done((bf16[288,256]{1,0:T(8,128)(2,1)S(1)}, bf16[288,256]{1,0:T(8,128)(2,1)}, u32[]{:S(2)}) %copy-start.2) | copy-done | bytes 147480
  3.8 0.0 copy-start.3
  3.8 0.9 %copy-done.3 = bf16[1,176,256]{2,1,0:T(8,128)(2,1)S(1)} copy-done((bf16[1,176,256]{2,1,0:T(8,128)(2,1)S(1)}, bf16[1,176,256]{2,1,0:T(8,128)(2,1)}, u32[]{:S(2)}) %copy-start.3) | copy-done | bytes 90136
  4.7 26.5 %fused_attention.1 = bf16[176,2048]{1,0:T(8,128)(2,1)S(1)} custom-call(bf16[176,2048]{1,0:T(8,128)(2,1)S(1)} %bitcast.8, bf16[176,256]{1,0:T(8,128)(2,1)S(1)} %bitcast.9, bf16[176,2304]{1,0:T(8,128)(2,1)S(1)} %bitcast.7, bf16[288,256]{1,0:T(8,128)(2,1)S(1)} %copy-done.2, f32[1,128]{1,0:T(1,128)S(1)} %bitcast.10, f32[1,128]{1,0:T(1,128)S(1)} %bitcast.11), custom_call_target="tpu_custom_call" | custom-call | tf_op jit(solution)/shard_map/fused_attention/pallas_call | solution.py:228
  31.2 0.9 %copy.8 = bf16[1,176,2048]{2,1,0:T(8,128)(2,1)} copy(bf16[1,176,2048]{2,1,0:T(8,128)(2,1)S(1)} %bitcast.6) | data formatting | bytes 1441792
Async XLA Ops:
  0.0 0.7 %copy-start.4 = (f32[128]{0:T(128)S(1)}, f32[128]{0:T(128)}, u32[]{:S(2)}) copy-start(f32[128]{0:T(128)} %param.10) | copy-start | bytes 1540
  0.0 0.7 %copy-start.5 = (f32[128]{0:T(128)S(1)}, f32[128]{0:T(128)}, u32[]{:S(2)}) copy-start(f32[128]{0:T(128)} %param.11) | copy-start | bytes 1540
  0.7 1.1 %copy-start = (bf16[1,176,2304]{2,1,0:T(8,128)(2,1)S(1)}, bf16[1,176,2304]{2,1,0:T(8,128)(2,1)}, u32[]{:S(2)}) copy-start(bf16[1,176,2304]{2,1,0:T(8,128)(2,1)} %param.8) | copy-start | bytes 2433028
  1.8 1.1 %copy-start.1 = (bf16[1,176,2048]{2,1,0:T(8,128)(2,1)S(1)}, bf16[1,176,2048]{2,1,0:T(8,128)(2,1)}, u32[]{:S(2)}) copy-start(bf16[1,176,2048]{2,1,0:T(8,128)(2,1)} %param.6) | copy-start | bytes 2162692
  2.9 0.9 %copy-start.2 = (bf16[288,256]{1,0:T(8,128)(2,1)S(1)}, bf16[288,256]{1,0:T(8,128)(2,1)}, u32[]{:S(2)}) copy-start(bf16[288,256]{1,0:T(8,128)(2,1)} %w_hbm.1) | copy-start | bytes 442372
  3.8 0.9 %copy-start.3 = (bf16[1,176,256]{2,1,0:T(8,128)(2,1)S(1)}, bf16[1,176,256]{2,1,0:T(8,128)(2,1)}, u32[]{:S(2)}) copy-start(bf16[1,176,256]{2,1,0:T(8,128)(2,1)} %param.7) | copy-start | bytes 270340

commit v3 on v2

--- a/solution.py
+++ b/solution.py
@@ -225,6 +225,8 @@
     ]
     held = sum(math.prod(shape) * jnp.dtype(kind).itemsize for shape, kind in buffers)
     limit = min(60 * 2 ** 20, held + held // 4 + 8 * rows * length * 4 + 4 * 2 ** 20)
+    operands = (queries[0], keys[0], tokens[0], w_value, q_gain[None], k_gain[None])
+    operands = [pltpu.with_memory_space_constraint(a, pltpu.HBM) for a in operands]
     out = pl.pallas_call(
         functools.partial(kernel, n_sp, n_dp),
         out_shape=jax.ShapeDtypeStruct((rows, QH * HD), bf16),
@@ -251,7 +253,7 @@
             collective_id=0, has_side_effects=True, vmem_limit_bytes=limit
         ),
         name="fused_attention",
-    )(queries[0], keys[0], tokens[0], w_value, q_gain[None], k_gain[None])
+    )(*operands)
     return out[None]
 
 

time: 32.3 us -> 27.5 us (0.85)
  local copies, waits for them, and re-layouts: 5.58 us -> 0.86 us
    unnamed x13 -> x1, local copies, waits for them, and re-layouts: 5.58 us -> 0.86 us
where the time goes in v3:
time: 27.5 us; the launch traced here: 27.3 us
  Pallas kernels  26.5 us (96%)
  local copies, waits for them, and re-layouts  0.86 us (3%)
    pallas_call x1, Pallas kernels, per_device(): pl.pallas_call(functools.partial(kernel, n_sp, n_dp), out_shape=jax.Shape...  26.5 us
    unnamed x1, local copies, waits for them, and re-layouts  0.86 us

profile of v3, /device:TPU:1, one launch (start us, length us, event | category | flops | bytes accessed | tf_op | source)
XLA Modules:
  0.0 27.3 jit_solution(14018054610067176823)
XLA Ops:
  0.0 26.5 %fused_attention.1 = bf16[176,2048]{1,0:T(8,128)(2,1)S(1)} custom-call(bf16[176,2048]{1,0:T(8,128)(2,1)} %bitcast.8, bf16[176,256]{1,0:T(8,128)(2,1)} %bitcast.9, bf16[176,2304]{1,0:T(8,128)(2,1)} %bitcast.7, bf16[288,256]{1,0:T(8,128)(2,1)} %w_hbm.1, f32[1,128]{1,0:T(1,128)} %bitcast.10, f32[1,128]{1,0:T(1,128)} %bitcast.11), custom_call_target="tpu_custom_call" | custom-call | tf_op jit(solution)/shard_map/fused_attention/pallas_call | solution.py:230
  26.5 0.9 %copy.8 = bf16[1,176,2048]{2,1,0:T(8,128)(2,1)} copy(bf16[1,176,2048]{2,1,0:T(8,128)(2,1)S(1)} %bitcast.6) | data formatting | bytes 1441792

commit v4 on v3

--- a/solution.py
+++ b/solution.py
@@ -22,6 +22,17 @@
     while size * size * 4 <= n and n % (size * 2) == 0:
         size *= 2
     return size
+
+
+def partner(index, d, n):
+    if n & (n - 1):
+        return (index + d) % n
+    bit = 1
+    while bit <= d:
+        if d & bit:
+            index = index + bit - 2 * bit * (index // bit % 2)
+        bit *= 2
+    return index
 
 
 def kernel(
@@ -46,7 +57,7 @@
     def token_part(core):
         return tok.at[pl.ds(pl.multiple_of(core * rows, 16), rows), :]
 
-    z_peers = [((z + d) % n_z) for d in range(1, n_z)]
+    z_peers = [partner(z, d, n_z) for d in range(1, n_z)]
     x_peers = [((x + d) % n_x) for d in range(1, n_x)]
     y_peers = [((y + d) % n_y) for d in range(1, n_y)]
 
@@ -127,10 +138,22 @@
     for h in range(QH):
         qrot[h] = norm_rot(q_in[:, h * HD:(h + 1) * HD], qg_ref[...])
 
+    def arrived(d):
+        remote(block(d), block(d), w_z.at[0], w_recv.at[d], (sp, d)).wait_recv()
+
+    def relay(i):
+        d = z_peers[i] * n_x + x
+        arrived(d)
+        for k, xp in enumerate(x_peers):
+            send(block(d), block(d), w_x.at[i + 1, k], w_recv.at[d], (sp, z * n_x + xp))
+
+    relays = [functools.partial(relay, i) for i in range(n_z - 1)]
     for i, yp in enumerate(y_peers):
         j = yp * 2 + c
         remote(at(kbuf, j), at(kbuf, j), k_send.at[0], k_recv.at[yp], (j, dp)).wait_recv()
         send(at(kbuf, j), at(kbuf, j), k_fwd.at[i], k_frecv.at[yp], (sib, dp))
+    for step_on in relays[:1]:
+        step_on()
     for yp in [y] + y_peers:
         j = yp * 2 + 1 - c
         remote(at(kbuf, j), at(kbuf, j), k_send.at[0], k_frecv.at[yp], (sib, dp)).wait_recv()
@@ -145,20 +168,10 @@
         e = jnp.exp2((s - jnp.max(s, axis=-1, keepdims=True)) * scale)
         prob[h] = (e * (1.0 / jnp.sum(e, axis=-1, keepdims=True))).astype(jnp.bfloat16)
 
-    def arrived(d):
-        remote(block(d), block(d), w_z.at[0], w_recv.at[d], (sp, d)).wait_recv()
-
-    def relay(i):
-        d = z_peers[i] * n_x + x
-        arrived(d)
-        for k, xp in enumerate(x_peers):
-            send(block(d), block(d), w_x.at[i + 1, k], w_recv.at[d], (sp, z * n_x + xp))
-
-    order = sorted(range(n_z - 1), key=lambda i: min(i + 1, n_z - 1 - i))
-    relays = [functools.partial(relay, i) for i in order]
+    relays = relays[1:]
     done = 0
     for part in range(GROUP // 2):
-        count = len(relays) * (part + 1) // (GROUP // 2)
+        count = len(relays) * part // (GROUP // 2 - 1) if part != 1 else -(-len(relays) // 2)
         for step_on in relays[done:count]:
             step_on()
         done = count
@@ -169,7 +182,7 @@
             def _(h, g=g):
                 weights(h, g)
 
-    for zz in [z] + [z_peers[i] for i in order]:
+    for zz in [z] + z_peers:
         for xp in x_peers:
             arrived(zz * n_x + xp)
     theirs = token_part(1 - c)
@@ -186,14 +199,19 @@
         there = chip(c, yp)
         remote(there, there, v_send.at[0], v_recv.at[yp], (yp * 2 + c, dp)).wait_recv()
         send(there, there, v_fwd.at[i], v_frecv.at[yp], (sib, dp))
+
+    def attend(core):
+        for i in range(GROUP):
+            h = core * GROUP + i
+            out_ref[:, pl.ds(pl.multiple_of(h * HD, HD), HD)] = jnp.dot(
+                prob[h], vbuf[core], preferred_element_type=jnp.float32
+            ).astype(jnp.bfloat16)
+
+    attend(c)
     for yp in [y] + y_peers:
         there = chip(1 - c, yp)
         remote(there, there, v_send.at[0], v_frecv.at[yp], (sib, dp)).wait_recv()
-
-    for h in range(QH):
-        out_ref[:, h * HD:(h + 1) * HD] = jnp.dot(
-            prob[h], vbuf[h // GROUP], preferred_element_type=jnp.float32
-        ).astype(jnp.bfloat16)
+    attend(1 - c)
     for copy in pending:
         copy.wait_send()
 

time: 27.5 us -> 27.1 us (0.985); the launches traced: 27.3 us -> 26.6 us
  Pallas kernels: 26.5 us -> 25.8 us
    pallas_call x1, Pallas kernels: 26.5 us -> 25.8 us  [per_device(): pl.pallas_call(functools.partial(kernel, n_sp, n_dp), out_shape=jax.Shape...]
where the time goes in v4:
time: 27.1 us; the launch traced here: 26.6 us
  Pallas kernels  25.8 us (95%)
  local copies, waits for them, and re-layouts  0.86 us (3%)
    pallas_call x1, Pallas kernels, per_device(): pl.pallas_call(functools.partial(kernel, n_sp, n_dp), out_shape=jax.Shape...  25.8 us
    unnamed x1, local copies, waits for them, and re-layouts  0.86 us

profile of v4, /device:TPU:1, one launch (start us, length us, event | category | flops | bytes accessed | tf_op | source)
XLA Modules:
  0.0 26.6 jit_solution(11923924750088920135)
XLA Ops:
  0.0 25.8 %fused_attention.1 = bf16[176,2048]{1,0:T(8,128)(2,1)S(1)} custom-call(bf16[176,2048]{1,0:T(8,128)(2,1)} %bitcast.8, bf16[176,256]{1,0:T(8,128)(2,1)} %bitcast.9, bf16[176,2304]{1,0:T(8,128)(2,1)} %bitcast.7, bf16[288,256]{1,0:T(8,128)(2,1)} %w_hbm.1, f32[1,128]{1,0:T(1,128)} %bitcast.10, f32[1,128]{1,0:T(1,128)} %bitcast.11), custom_call_target="tpu_custom_call" | custom-call | tf_op jit(solution)/shard_map/fused_attention/pallas_call | solution.py:248
  25.8 0.9 %copy.8 = bf16[1,176,2048]{2,1,0:T(8,128)(2,1)} copy(bf16[1,176,2048]{2,1,0:T(8,128)(2,1)S(1)} %bitcast.6) | data formatting | bytes 1441792

commit v5 on v4

--- a/solution.py
+++ b/solution.py
@@ -116,10 +116,6 @@
         return ref.at[pl.ds(pl.multiple_of(s * rows, 16), rows), :]
 
     own = pl.ds(pl.multiple_of(sp * rows, 16), rows)
-    loads[0].wait()
-    loads[1].wait()
-    for g in range(KVH):
-        kbuf[own, g * HD:(g + 1) * HD] = norm_rot(k_in[:, g * HD:(g + 1) * HD], kg_ref[...])
     loads[2].wait()
 
     pl.semaphore_wait(barrier, n_z - 1 + n_x - 1 + n_y)
@@ -127,6 +123,10 @@
         send(block(dp), block(dp), w_z.at[i], w_recv.at[dp], (sp, zp * n_x + x))
     for i, xp in enumerate(x_peers):
         send(block(dp), block(dp), w_x.at[0, i], w_recv.at[dp], (sp, z * n_x + xp))
+    loads[0].wait()
+    loads[1].wait()
+    for g in range(KVH):
+        kbuf[own, g * HD:(g + 1) * HD] = norm_rot(k_in[:, g * HD:(g + 1) * HD], kg_ref[...])
     for i, yp in enumerate(y_peers):
         send(at(kbuf, sp), at(kbuf, sp), k_send.at[i], k_recv.at[y], (yp * 2 + c, dp))
     send(at(kbuf, sp), at(kbuf, sp), k_send.at[n_y - 1], k_frecv.at[y], (sib, dp))

time: 27.1 us -> 27.4 us (1.011)
  Pallas kernels: 25.8 us -> 26.1 us
    pallas_call x1, Pallas kernels: 25.8 us -> 26.1 us  [per_device(): pl.pallas_call(functools.partial(kernel, n_sp, n_dp), out_shape=jax.Shape...]
where the time goes in v5:
time: 27.4 us; the launch traced here: 27 us
  Pallas kernels  26.1 us (95%)
  local copies, waits for them, and re-layouts  0.86 us (3%)
    pallas_call x1, Pallas kernels, per_device(): pl.pallas_call(functools.partial(kernel, n_sp, n_dp), out_shape=jax.Shape...  26.1 us
    unnamed x1, local copies, waits for them, and re-layouts  0.86 us

profile of v5, /device:TPU:1, one launch (start us, length us, event | category | flops | bytes accessed | tf_op | source)
XLA Modules:
  0.0 27.0 jit_solution(749417818707835806)
XLA Ops:
  0.0 26.1 %fused_attention.1 = bf16[176,2048]{1,0:T(8,128)(2,1)S(1)} custom-call(bf16[176,2048]{1,0:T(8,128)(2,1)} %bitcast.8, bf16[176,256]{1,0:T(8,128)(2,1)} %bitcast.9, bf16[176,2304]{1,0:T(8,128)(2,1)} %bitcast.7, bf16[288,256]{1,0:T(8,128)(2,1)} %w_hbm.1, f32[1,128]{1,0:T(1,128)} %bitcast.10, f32[1,128]{1,0:T(1,128)} %bitcast.11), custom_call_target="tpu_custom_call" | custom-call | tf_op jit(solution)/shard_map/fused_attention/pallas_call | solution.py:248
  26.1 0.9 %copy.8 = bf16[1,176,2048]{2,1,0:T(8,128)(2,1)} copy(bf16[1,176,2048]{2,1,0:T(8,128)(2,1)S(1)} %bitcast.6) | data formatting | bytes 1441792
